TPU v7x, 512 devices: a whole 4x8x8 slice. The times are simulated.
512 devices in a mesh: sp: 32 (over z, x), tp: 16 (over y, core).
Axes of the slice: x: 4, y: 8, z: 8, core: 2. Of those that a mesh axis runs over, the one named last changes fastest.
Arguments:
- latent: bfloat16 [16384, 2048], P('sp'), may hold values from -6 to 6
- context: bfloat16 [512, 2048], P('sp'), may hold values from -6 to 6
- condition: bfloat16 [2048], replicated, may hold values from -6 to 6
- context_condition: bfloat16 [2048], replicated, may hold values from -6 to 6
- shift_weight: bfloat16 [2048, 2048], P('sp', 'tp'), may hold values from -0.125 to 0.125
- scale_weight: bfloat16 [2048, 2048], P('sp', 'tp'), may hold values from -0.125 to 0.125
- mod_gate_weight: bfloat16 [2048, 2048], P('sp', 'tp'), may hold values from -0.5 to 0.5
- norm_gain: bfloat16 [2048], replicated, may hold values from 0.099609375 to 1.8984375
- query_weight: bfloat16 [2048, 2048], P(None, 'tp'), may hold values from -0.125 to 0.125
- key_weight: bfloat16 [2048, 2048], P(None, 'tp'), may hold values from -0.125 to 0.125
- value_weight: bfloat16 [2048, 2048], P(None, 'tp'), may hold values from -0.125 to 0.125
- gate_weight: bfloat16 [2048, 2048], P(None, 'tp'), may hold values from -0.125 to 0.125
- forward_decay: float32 [16], P('tp'), may hold values from 0 to 1, as said below
- backward_decay: float32 [16], P('tp'), may hold values from 0 to 1, as said below
- out_weight: bfloat16 [2048, 2048], P('tp'), may hold values from -0.125 to 0.125
Outputs:
- mixed: bfloat16 [16384, 2048], P('sp')
Inputs may be any that keep to these rules, and one draw needn't show every extreme that they name: `forward_decay`: each head's rate is positive. `backward_decay`: each head's rate is positive.
All inputs are finite; a program needn't handle non-finite values.
Results may differ from a plain program's by a relative error of at most 0.015.
Values may be sent and summed in bfloat16 or wider, within the bound.
No kernel may reach another device: no remote copies, remote signals or barrier semaphores. Data moves between devices by JAX's collectives and lax.ppermute only.
A program may use at most 64 MiB of HBM per device.

v0:
```python
import jax
import jax.numpy as jnp
from jax import lax
from jax.sharding import Mesh
from jax.sharding import PartitionSpec as P

HEAD_DIM = 128
GRID_W = 64
SP = ("sp_0", "sp_1")
EPS = 1e-06
THETA = 10000.0
CONTEXT_LIFT = 3.0
TOP_PRECISION = lax.Precision.HIGHEST


def sent_to_all(x, axis):
    copies = jnp.broadcast_to(x, (lax.axis_size(axis), *x.shape))
    return lax.all_to_all(copies, axis, split_axis=0, concat_axis=0, tiled=True)


def taken_together(x, axis):
    everything = sent_to_all(x, axis)
    return jnp.sum(everything, axis=0)


def in_one(arrays, axis):
    ravelled, at, finished = (jnp.concatenate([a.reshape(-1) for a in arrays]), 0, [])
    total = lax.psum(ravelled, axis)
    for a in arrays:
        finished.append(total[at : at + a.size].reshape(a.shape))
        at += a.size
    return tuple(finished)


def filled_with(x, identity):
    return jax.tree.map(
        lambda a, e: jnp.broadcast_to(jnp.asarray(e, a.dtype), a.shape), x, identity
    )


def all_in_one(x, axis):
    leaves = jax.tree.leaves(x)
    order = sorted(range(len(leaves)), key=lambda k: -leaves[k].size)
    width = (1, *leaves[order[0]].shape)[-1]
    lines = [
        jnp.pad(leaves[k].reshape(-1), (0, -leaves[k].size % width)).reshape(-1, width)
        for k in order
    ]
    both, at, found = (lax.all_gather(jnp.concatenate(lines), axis), 0, {})
    for k, line in zip(order, lines):
        slab = both[:, at : at + len(line)].reshape(len(both), -1)
        found[k] = slab[:, : leaves[k].size].reshape(-1, *leaves[k].shape)
        at += len(line)
    numbers = iter(range(len(leaves)))
    return jax.tree.map(lambda _: found[next(numbers)], x)


def prefix_by_axis(x, axes, combine, identity, reverse):
    before = start = filled_with(x, identity)
    total = x
    for axis in reversed(axes):
        length, mine = (lax.axis_size(axis), lax.axis_index(axis))
        pieces = all_in_one(total, axis)
        inside, total = (start, start)
        for k in reversed(range(length)) if reverse else range(length):
            passed = k > mine if reverse else k < mine
            total = combine(total, jax.tree.map(lambda part: part[k], pieces))
            inside = jax.tree.map(lambda new, old: jnp.where(passed, new, old), total, inside)
        before = combine(inside, before)
    return before


def laid_out(parts, dim):
    dims = list(parts.shape[1:])
    dims[dim] *= parts.shape[0]
    return jnp.moveaxis(parts, 0, dim).reshape(dims)


def collect(x, axis, dim):
    return laid_out(sent_to_all(x, axis), dim)


def modulated(token_rows, norm_gain, shifts, scales):
    values = token_rows.astype(jnp.float32)
    values = values * lax.rsqrt(jnp.mean(values * values, axis=-1, keepdims=True) + EPS)
    values = values * norm_gain.astype(jnp.float32)
    return (values * (1.0 + scales) + shifts).astype(jnp.bfloat16)


def rope_half(portion, positions):
    quarter = portion.shape[-1] // 2
    frequency = THETA ** (-jnp.arange(quarter, dtype=jnp.float32) / quarter)
    angles = positions[:, None, None] * frequency
    cosine = jnp.cos(angles)
    sine_table = jnp.sin(angles)
    leading = portion[..., :quarter]
    trailing = portion[..., quarter:]
    return jnp.concatenate(
        [leading * cosine - trailing * sine_table, leading * sine_table + trailing * cosine],
        axis=-1,
    )


def rotate(values, grid_row, grid_column):
    half_width = values.shape[-1] // 2
    return jnp.concatenate(
        [
            rope_half(values[..., :half_width], grid_row),
            rope_half(values[..., half_width:], grid_column),
        ],
        axis=-1,
    )


def combine(earlier, later):
    return (earlier[0] * later[0], later[0][:, None, None] * earlier[1] + later[1])


def local(
    latent,
    context,
    condition,
    context_condition,
    shift_weight,
    scale_weight,
    mod_gate_weight,
    norm_gain,
    query_weight,
    key_weight,
    value_weight,
    gate_weight,
    forward_decay,
    backward_decay,
    out_weight,
):
    sp_index = lax.axis_index(SP)
    tp_index = lax.axis_index("tp")
    sp_count = lax.axis_size(SP)
    tp_count = lax.axis_size("tp")
    tokens_here = latent.shape[0]
    local_rows = tokens_here // tp_count
    mod_rows = shift_weight.shape[0]
    activation = jax.nn.silu(jnp.stack([condition, context_condition]).astype(jnp.float32)).astype(
        jnp.bfloat16
    )
    own_part = lax.dynamic_slice_in_dim(activation, sp_index * mod_rows, mod_rows, 1)
    partial_value = jnp.stack(
        [
            jnp.dot(own_part, matrix, preferred_element_type=jnp.float32)
            for matrix in (shift_weight, scale_weight, mod_gate_weight)
        ]
    )
    summed = taken_together(partial_value, SP)
    modulation = lax.all_gather(summed, "tp", axis=2, tiled=True)
    hidden = modulated(latent, norm_gain, modulation[0, 0], modulation[1, 0])
    context_hidden = modulated(context, norm_gain, modulation[0, 1], modulation[1, 1])
    local_width = query_weight.shape[1]
    head_count = local_width // HEAD_DIM
    stacked = jnp.concatenate([query_weight, key_weight, value_weight, gate_weight], axis=1)
    projected = jnp.dot(hidden, stacked, preferred_element_type=jnp.float32).astype(jnp.bfloat16)
    queries = projected[:, :local_width]
    keys_out = projected[:, local_width : 2 * local_width]
    values_out = projected[:, 2 * local_width : 3 * local_width]
    out_gates = projected[:, 3 * local_width :]
    context_pairs = jnp.dot(
        context_hidden,
        stacked[:, local_width : 3 * local_width],
        preferred_element_type=jnp.float32,
    ).astype(jnp.bfloat16)

    def to_heads(values):
        return values.astype(jnp.float32).reshape(values.shape[0], head_count, HEAD_DIM)

    positions = sp_index * tokens_here + jnp.arange(tokens_here, dtype=jnp.int32)
    grid_row = (positions // GRID_W).astype(jnp.float32)
    grid_column = (positions % GRID_W).astype(jnp.float32)
    key_scale = HEAD_DIM ** (-0.5)
    query_heads = jnp.transpose(rotate(to_heads(queries), grid_row, grid_column), (1, 0, 2))
    key_heads = (
        jnp.transpose(rotate(to_heads(keys_out), grid_row, grid_column), (1, 0, 2)) * key_scale
    )
    value_heads = jnp.transpose(to_heads(values_out), (1, 0, 2))
    log_forward = -forward_decay
    log_backward = -backward_decay
    context_rows = context.shape[0]
    context_total = context_rows * sp_count
    context_index = (sp_index * context_rows + jnp.arange(context_rows, dtype=jnp.int32)).astype(
        jnp.float32
    )
    weight_forward = jnp.exp(log_forward[:, None] * (context_total - 1.0 - context_index)[None, :])
    weight_backward = jnp.exp(log_backward[:, None] * context_index[None, :])
    context_key_heads = to_heads(context_pairs[:, :local_width]) * (key_scale * CONTEXT_LIFT)
    context_value_heads = to_heads(context_pairs[:, local_width:])
    context_forward = jnp.einsum(
        "hc,chd,che->hde",
        weight_forward,
        context_key_heads,
        context_value_heads,
        precision=TOP_PRECISION,
    )
    context_backward = jnp.einsum(
        "hc,chd,che->hde",
        weight_backward,
        context_key_heads,
        context_value_heads,
        precision=TOP_PRECISION,
    )
    context_forward, context_backward = in_one((context_forward, context_backward), SP)
    offsets = jnp.arange(tokens_here, dtype=jnp.float32)
    distance = offsets[:, None] - offsets[None, :]
    mixing = jnp.where(
        distance >= 0, jnp.exp(log_forward[:, None, None] * jnp.maximum(distance, 0.0)), 0.0
    )
    mixing = mixing + jnp.where(
        distance <= 0, jnp.exp(log_backward[:, None, None] * jnp.maximum(-distance, 0.0)), 0.0
    )
    score_matrix = (
        jnp.einsum("htd,hsd->hts", query_heads, key_heads, precision=TOP_PRECISION) * mixing
    )
    local_out = jnp.einsum("hts,hse->hte", score_matrix, value_heads, precision=TOP_PRECISION)
    tail_forward = jnp.exp(log_forward[:, None] * (tokens_here - 1.0 - offsets)[None, :])
    head_backward = jnp.exp(log_backward[:, None] * offsets[None, :])
    own_forward = jnp.einsum(
        "ht,htd,hte->hde", tail_forward, key_heads, value_heads, precision=TOP_PRECISION
    )
    own_backward = jnp.einsum(
        "ht,htd,hte->hde", head_backward, key_heads, value_heads, precision=TOP_PRECISION
    )
    span_forward = jnp.exp(log_forward * tokens_here)
    span_backward = jnp.exp(log_backward * tokens_here)
    identity = (jnp.ones_like(span_forward), jnp.zeros_like(own_forward))
    before = prefix_by_axis((span_forward, own_forward), SP, combine, identity, False)
    after = prefix_by_axis((span_backward, own_backward), SP, combine, identity, True)
    device_start = (sp_index * tokens_here).astype(jnp.float32)
    device_rest = ((sp_count - 1 - sp_index) * tokens_here).astype(jnp.float32)
    incoming_forward = (
        before[1] + jnp.exp(log_forward * device_start)[:, None, None] * context_forward
    )
    incoming_backward = (
        after[1] + jnp.exp(log_backward * device_rest)[:, None, None] * context_backward
    )
    read_forward = jnp.exp(log_forward[:, None] * (offsets + 1.0)[None, :])[
        :, :, None
    ] * jnp.einsum("htd,hde->hte", query_heads, incoming_forward, precision=TOP_PRECISION)
    read_backward = jnp.exp(log_backward[:, None] * (tokens_here - offsets)[None, :])[
        :, :, None
    ] * jnp.einsum("htd,hde->hte", query_heads, incoming_backward, precision=TOP_PRECISION)
    retained = local_out + read_forward + read_backward
    retained = retained * lax.rsqrt(jnp.mean(retained * retained, axis=-1, keepdims=True) + EPS)
    merged = jnp.transpose(retained, (1, 0, 2)).reshape(tokens_here, local_width)
    heads_out = (jax.nn.silu(out_gates.astype(jnp.float32)) * merged).astype(jnp.bfloat16)
    projection = lax.psum_scatter(
        jnp.dot(heads_out, out_weight, preferred_element_type=jnp.float32),
        "tp",
        scatter_dimension=0,
        tiled=True,
    )
    own_latent = lax.dynamic_slice_in_dim(latent, tp_index * local_rows, local_rows, 0)
    finished = (own_latent.astype(jnp.float32) + modulation[2, 0] * projection).astype(jnp.bfloat16)
    return collect(finished, "tp", 0)


def solution(mesh):
    torus = Mesh(mesh.devices.reshape(8, 4, mesh.shape["tp"]), ("sp_0", "sp_1", "tp"))
    in_specs = (
        P(SP, None),
        P(SP, None),
        P(),
        P(),
        P(SP, "tp"),
        P(SP, "tp"),
        P(SP, "tp"),
        P(),
        P(None, "tp"),
        P(None, "tp"),
        P(None, "tp"),
        P(None, "tp"),
        P("tp"),
        P("tp"),
        P("tp", None),
    )
    out_specs = P(SP, None)
    return jax.shard_map(local, mesh=torus, in_specs=in_specs, out_specs=out_specs, check_vma=False)
```

profile of v0, /device:TPU:1, one launch (start us, length us, event | category | flops | bytes accessed | tf_op | source)
XLA Modules:
  0.0 352.9 jit_solution(17837896909596042663)
XLA Ops:
  6.5 0.0 copy-start
  6.5 0.0 copy-start.1
  6.5 0.0 copy-start.8
  6.5 0.8 stack.21
  7.4 0.7 stack.22
  8.1 0.9 convolution_bitcast_fusion.4
  9.0 0.9 convolution_bitcast_fusion.3
  9.9 0.9 convolution_bitcast_fusion.2
  10.9 0.7 broadcast_in_dim.10
  11.5 13.7 %all-to-all-start = ((f32[32,3,2,128]{3,2,1,0:T(2,128)}), f32[32,3,2,128]{3,2,1,0:T(2,128)S(1)}, u32[]{:S(2)}, u32[]{:S(2)}) async-start(f32[32,3,2,128]{3,2,1,0:T(2,128)} %broadcast_in_dim.10), calls=%async_computation | async-start | bytes 196608 | tf_op jit(solution)/shard_map/all_to_all | solution.py:18
  25.3 0.0 all-reduce.6.cloned.1.call-start
  27.0 1.0 fusion.45
  28.0 2.1 fusion
  30.0 0.7 convert_element_type.83
  30.7 3.6 %all-to-all-done = f32[32,3,2,128]{3,2,1,0:T(2,128)S(1)} async-done(((f32[32,3,2,128]{3,2,1,0:T(2,128)}), f32[32,3,2,128]{3,2,1,0:T(2,128)S(1)}, u32[]{:S(2)}, u32[]{:S(2)}) %all-to-all-start) | async-done | bytes 98336 | tf_op jit(solution)/shard_map/all_to_all | solution.py:18
  34.4 0.1 reduce_sum.36
  34.4 19.6 %all_gather.27 = f32[3,2,2048]{2,1,0:T(2,128)S(1)} all-gather(f32[3,2,128]{2,1,0:T(2,128)S(1)} %reduce_sum.36), channel_id=1, replica_groups=mesh['sp_0'=8,'sp_1'=4,'tp'=16] {'tp'}, dimensions={2}, use_global_device_ids=true | all-gather | bytes 52224 | tf_op jit(solution)/shard_map/all_gather | solution.py:154
  54.1 1.5 convolution_convert_fusion
  55.6 0.3 convolution_bitcast_fusion.1
  55.9 0.3 convolution_bitcast_fusion
  56.2 0.7 pad_maximum_fusion
  56.9 0.0 all-reduce.6.cloned.1.call-update
  56.9 0.0 reduce-scatter.2.cloned.1.call-start
  57.0 0.0 copy-done.1
  57.0 0.0 copy-done.8
  57.0 2.9 fusion.18
  59.9 0.0 copy-start.4
  59.9 0.1 fusion.53
  60.0 0.6 fusion.82
  60.5 0.0 copy-start.5
  60.5 0.0 copy-start.6
  60.6 0.0 copy-start.7
  60.6 0.3 fusion.40
  60.8 0.3 fusion.42
  61.1 9.4 %all-gather.4 = f32[4,129,128]{2,1,0:T(8,128)S(1)} all-gather(f32[1,129,128]{2,1,0:T(8,128)S(1)} %maximum_bitcast_fusion.4), channel_id=2, replica_groups=mesh['sp_0'=8,'sp_1'=4,'tp'=16] {'sp_1'}, dimensions={0}, use_global_device_ids=true | all-gather | bytes 330240 | tf_op jit(solution)/shard_map/all_gather | solution.py:49
  70.6 0.6 fusion.227
  74.4 9.7 %all-gather.6 = f32[4,129,128]{2,1,0:T(8,128)S(1)} all-gather(f32[1,129,128]{2,1,0:T(8,128)S(1)} %maximum_bitcast_fusion.6), channel_id=4, replica_groups=mesh['sp_0'=8,'sp_1'=4,'tp'=16] {'sp_1'}, dimensions={0}, use_global_device_ids=true | all-gather | bytes 330240 | tf_op jit(solution)/shard_map/all_gather | solution.py:49
  84.1 0.6 fusion.226
  89.2 2.0 fusion.233
  91.1 19.6 %all-gather.7 = f32[8,129,128]{2,1,0:T(8,128)S(1)} all-gather(f32[1,129,128]{2,1,0:T(8,128)S(1)} %maximum_bitcast_fusion.7), channel_id=5, replica_groups=mesh['sp_0'=8,'sp_1'=4,'tp'=16] {'sp_0'}, dimensions={0}, use_global_device_ids=true | all-gather | bytes 594432 | tf_op jit(solution)/shard_map/all_gather | solution.py:49
  110.7 0.0 copy-start.2
  110.7 0.7 fusion.224
  111.4 1.9 fusion.234
  113.3 20.3 %all-gather.5 = f32[8,129,128]{2,1,0:T(8,128)S(1)} all-gather(f32[1,129,128]{2,1,0:T(8,128)S(1)} %maximum_bitcast_fusion.5), channel_id=3, replica_groups=mesh['sp_0'=8,'sp_1'=4,'tp'=16] {'sp_0'}, dimensions={0}, use_global_device_ids=true | all-gather | bytes 594432 | tf_op jit(solution)/shard_map/all_gather | solution.py:49
  133.7 0.7 fusion.225
  135.6 0.0 copy-done.2
  135.6 0.0 copy-done.3
  135.6 1.5 convolution_multiply_fusion
  137.2 0.0 copy-done.4
  137.2 0.0 copy-done.5
  137.2 0.0 copy-done.6
  137.2 0.0 copy-done.7
  137.2 0.7 fusion.62
  137.9 61.9 %all-reduce.6.cloned.1.call-done = f32[32768]{0:T(1024)} async-done(((f32[32768]{0:T(1024)}), f32[32768]{0:T(1024)}) %all-reduce.6.cloned.1.call-update) | async-done | bytes 131088 | tf_op jit(solution)/shard_map/psum | solution.py:28
  199.9 8.0 %fusion.24 = f32[512,128]{0,1:T(8,128)S(1)} fusion(f32[512,128]{0,1:T(8,128)S(1)} %fusion.62, f32[512]{0:T(512)S(1)} %multiply_exponential_fusion.1, f32[32768]{0:T(1024)} %all-reduce.6.cloned.1.call-done, f32[8,129,128]{2,1,0:T(8,128)} %copy-done.3, f32[4,129,128]{2,1,0:T(8,128)S(1)} %all-gather.4, f32[512,1,32]{0,2,1:T(8,128)} %copy-done.5, ...), kind=kOutput, calls=%fused_computation.26 | convolution fusion | flops 101695488 | bytes 1847816 | tf_op jit(solution)/shard_map/htd,hde->hte/dot_general | solution.py:244
  207.9 8.0 %multiply_reduce_fusion = (f32[512]{0:T(512)S(1)}, f32[512,128]{0,1:T(8,128)S(1)}) fusion(f32[512,128]{0,1:T(8,128)S(1)} %fusion.24, f32[32768]{0:T(1024)} %all-reduce.6.cloned.1.call-done, f32[8,129,128]{2,1,0:T(8,128)} %copy-done.2, f32[4,129,128]{2,1,0:T(8,128)S(1)} %all-gather.6, f32[]{:T(128)} %bitcast.75, f32[]{:T(128)} %bitcast.76, f32[]{:T(128)} %bitcast.77, ...), kind=kOutput, calls=%fused_computation.53 | convolution fusion | flops 101826048 | bytes 1849864 | tf_op jit(solution)/shard_map/htd,hde->hte/dot_general | solution.py:247
  215.9 0.0 copy-done
  215.9 3.6 %fusion.50 = f32[512,2048]{1,0:T(8,128)} fusion(bf16[128,2048]{1,0:T(8,128)(2,1)S(1)} %copy-done, f32[512,128]{0,1:T(8,128)S(1)} %get-tuple-element.53, bf16[512,512]{0,1:T(8,128)(2,1)} %copy-done.4, f32[512]{0:T(512)S(1)} %add_rsqrt_fusion), kind=kOutput, calls=%fused_computation.66 | convolution fusion | flops 268959744 | bytes 5113856 | tf_op jit(solution)/shard_map/dot_general | solution.py:253
  219.5 0.0 reduce-scatter.2.cloned.1.call-update
  219.5 66.3 %reduce-scatter.2.cloned.1.call-done = f32[32,2048]{1,0:T(8,128)} async-done(((f32[512,2048]{1,0:T(8,128)}), f32[32,2048]{1,0:T(8,128)}) %reduce-scatter.2.cloned.1.call-update) | async-done | bytes 262160 | tf_op jit(solution)/shard_map/reduce_scatter | solution.py:252
  285.8 1.0 add_convert_fusion
  286.8 0.2 broadcast_in_dim.12
  287.1 57.7 %all_to_all.10 = bf16[16,32,2048]{2,1,0:T(8,128)(2,1)S(1)} all-to-all(bf16[16,32,2048]{2,1,0:T(8,128)(2,1)S(1)} %broadcast_in_dim.12), channel_id=1, replica_groups=mesh['sp_0'=8,'sp_1'=4,'tp'=16] {'tp'}, dimensions={0} | all-to-all | bytes 4194304 | tf_op jit(solution)/shard_map/all_to_all | solution.py:18
  344.8 1.3 copy.34
  (26 shorter events, 0.2 us)
Async XLA Ops:
  6.5 209.4 %copy-start = (bf16[128,2048]{1,0:T(8,128)(2,1)S(1)}, bf16[128,2048]{1,0:T(8,128)(2,1)}, u32[]{:S(2)}) copy-start(bf16[128,2048]{1,0:T(8,128)(2,1)} %param.29) | copy-start | bytes 1572868
  6.5 50.4 %copy-start.1 = (bf16[512,2048]{1,0:T(8,128)(2,1)S(1)}, bf16[512,2048]{1,0:T(8,128)(2,1)}, u32[]{:S(2)}) copy-start(bf16[512,2048]{1,0:T(8,128)(2,1)} %param.15) | copy-start | bytes 6291460
  6.5 50.4 %copy-start.8 = (bf16[2048,128]{1,0:T(8,128)(2,1)S(1)}, bf16[2048,128]{1,0:T(8,128)(2,1)}, u32[]{:S(2)}) copy-start(bf16[2048,128]{1,0:T(8,128)(2,1)} %param.25) | copy-start | bytes 1572868
  11.5 22.8 %all-to-all-start = ((f32[32,3,2,128]{3,2,1,0:T(2,128)}), f32[32,3,2,128]{3,2,1,0:T(2,128)S(1)}, u32[]{:S(2)}, u32[]{:S(2)}) async-start(f32[32,3,2,128]{3,2,1,0:T(2,128)} %broadcast_in_dim.10), calls=%async_computation | async-start | bytes 196608 | tf_op jit(solution)/shard_map/all_to_all | solution.py:18
  25.3 174.6 %all-reduce.6.cloned.1.call-start = ((), (), s32[]{:S(2)}) async-start(), calls=%async_computation.3 | async-start | bytes 262144 | tf_op jit(solution)/shard_map/psum | solution.py:28
  56.9 228.9 %reduce-scatter.2.cloned.1.call-start = ((), (), s32[]{:S(2)}) async-start(), calls=%async_computation.4 | async-start | bytes 4456448 | tf_op jit(solution)/shard_map/reduce_scatter | solution.py:252
  59.9 77.3 %copy-start.4 = (bf16[512,512]{0,1:T(8,128)(2,1)}, bf16[512,512]{0,1:T(8,128)(2,1)S(1)}, u32[]{:S(2)}) copy-start(bf16[512,512]{0,1:T(8,128)(2,1)S(1)} %fusion.18) | copy-start | bytes 1572868
  60.5 76.6 %copy-start.5 = (f32[512,1,32]{0,2,1:T(8,128)}, f32[512,1,32]{0,2,1:T(8,128)S(1)}, u32[]{:S(2)}) copy-start(f32[512,1,32]{0,2,1:T(8,128)S(1)} %get-tuple-element.25) | copy-start | bytes 196612
  60.5 76.6 %copy-start.6 = (f32[512,1,32]{0,2,1:T(8,128)}, f32[512,1,32]{0,2,1:T(8,128)S(1)}, u32[]{:S(2)}) copy-start(f32[512,1,32]{0,2,1:T(8,128)S(1)} %get-tuple-element.26) | copy-start | bytes 196612
  60.6 76.6 %copy-start.7 = (f32[512,1,32]{0,2,1:T(8,128)}, f32[512,1,32]{0,2,1:T(8,128)S(1)}, u32[]{:S(2)}) copy-start(f32[512,1,32]{0,2,1:T(8,128)S(1)} %get-tuple-element.27) | copy-start | bytes 196612
  110.7 24.9 %copy-start.2 = (f32[8,129,128]{2,1,0:T(8,128)}, f32[8,129,128]{2,1,0:T(8,128)S(1)}, u32[]{:S(2)}) copy-start(f32[8,129,128]{2,1,0:T(8,128)S(1)} %all-gather.7) | copy-start | bytes 1585156
  133.7 2.0 copy-start.3
Sparse Core Ops, SparseCore 0:
  57.0 142.7 all-reduce.5
  219.6 66.1 reduce-scatter.1
where the time goes:
time: 354 us; the launch traced here: 353 us
  blocking collectives  136 us (38%)
  waiting for transfers between devices  132 us (37%)
  matrix products  30.2 us (9%)
  between operations  24.2 us (7%)
  starting transfers between devices  13.8 us (4%)
  other arithmetic  10.1 us (3%)
  local copies, waits for them, and re-layouts  6.43 us (2%)
    reduce_scatter x1, waiting for transfers between devices, local(): lax.psum_scatter(jnp.dot(heads_out, out_weight, preferred_element_type=jn...  66.3 us
    psum x1, waiting for transfers between devices, in_one(): total = lax.psum(ravelled, axis)  61.9 us
    all_gather x4, blocking collectives, all_in_one(): both, at, found = (lax.all_gather(jnp.concatenate(lines), axis), 0, {})  59 us
    all_to_all x1, blocking collectives, sent_to_all(): return lax.all_to_all(copies, axis, split_axis=0, concat_axis=0, tiled=True)  57.7 us
    all_gather x1, blocking collectives, local(): modulation = lax.all_gather(summed, 'tp', axis=2, tiled=True)  19.6 us
    all_to_all x1, starting transfers between devices, sent_to_all(): return lax.all_to_all(copies, axis, split_axis=0, concat_axis=0, tiled=True)  13.7 us
    dot_general x1, matrix products, local(): jnp.einsum('htd,hde->hte', query_heads, incoming_forward, precision=TOP_P...  8.03 us
    dot_general x1, matrix products, local(): jnp.einsum('htd,hde->hte', query_heads, incoming_backward, precision=TOP_...  7.98 us
  transfers between devices with their start and end apart: 3, of which 3 were waited for; matrix products, arithmetic and copies ran while one was open for 5% of the time, Pallas kernels for 0%

commit v1 on v0

--- a/solution.py
+++ b/solution.py
@@ -151,7 +151,10 @@
         ]
     )
     summed = taken_together(partial_value, SP)
-    modulation = lax.all_gather(summed, "tp", axis=2, tiled=True)
+    size = lax.axis_size("tp")
+    blocks = jnp.stack([summed for _ in range(size)])
+    blocks = lax.all_to_all(blocks, "tp", split_axis=0, concat_axis=0)
+    modulation = jnp.concatenate(blocks, axis=2)
     hidden = modulated(latent, norm_gain, modulation[0, 0], modulation[1, 0])
     context_hidden = modulated(context, norm_gain, modulation[0, 1], modulation[1, 1])
     local_width = query_weight.shape[1]

time: 354 us -> 350 us (0.989)
  blocking collectives: 136 us -> 117 us
  starting transfers between devices: 13.8 us -> 23 us
  waiting for transfers between devices: 132 us -> 137 us
    all_gather x1 -> x0, blocking collectives: 19.6 us -> none  [local(): modulation = lax.all_gather(summed, 'tp', axis=2, tiled=True)]
    all_to_all x0 -> x1, starting transfers between devices: none -> 9.18 us  [local(): blocks = lax.all_to_all(blocks, 'tp', split_axis=0, concat_axis=0)]
    all_to_all x0 -> x1, waiting for transfers between devices: none -> 7.42 us  [local(): blocks = lax.all_to_all(blocks, 'tp', split_axis=0, concat_axis=0)]
  transfers between devices with their start and end apart: 3 -> 4, of which waited for: 3 -> 4; matrix products, arithmetic and copies ran while one was open for 5% -> 5% of each run, Pallas kernels for 0% -> 0%
where the time goes in v1:
time: 350 us; the launch traced here: 348 us
  waiting for transfers between devices  137 us (39%)
  blocking collectives  117 us (33%)
  matrix products  30.1 us (9%)
  between operations  24 us (7%)
  starting transfers between devices  23 us (7%)
  other arithmetic  10.1 us (3%)
  local copies, waits for them, and re-layouts  7.13 us (2%)
    reduce_scatter x1, waiting for transfers between devices, local(): lax.psum_scatter(jnp.dot(heads_out, out_weight, preferred_element_type=jn...  66.1 us
    all_gather x4, blocking collectives, all_in_one(): both, at, found = (lax.all_gather(jnp.concatenate(lines), axis), 0, {})  59.7 us
    psum x1, waiting for transfers between devices, in_one(): total = lax.psum(ravelled, axis)  59.5 us
    all_to_all x1, blocking collectives, sent_to_all(): return lax.all_to_all(copies, axis, split_axis=0, concat_axis=0, tiled=True)  57.6 us
    all_to_all x1, starting transfers between devices, sent_to_all(): return lax.all_to_all(copies, axis, split_axis=0, concat_axis=0, tiled=True)  13.7 us
    all_to_all x1, starting transfers between devices, local(): blocks = lax.all_to_all(blocks, 'tp', split_axis=0, concat_axis=0)  9.18 us
    dot_general x1, matrix products, local(): jnp.einsum('htd,hde->hte', query_heads, incoming_backward, precision=TOP_...  7.94 us
    dot_general x1, matrix products, local(): jnp.einsum('htd,hde->hte', query_heads, incoming_forward, precision=TOP_P...  7.92 us
  transfers between devices with their start and end apart: 4, of which 4 were waited for; matrix products, arithmetic and copies ran while one was open for 5% of the time, Pallas kernels for 0%

profile of v1, /device:TPU:1, one launch (start us, length us, event | category | flops | bytes accessed | tf_op | source)
XLA Modules:
  0.0 348.4 jit_solution(16608590982152766541)
XLA Ops:
  6.5 0.0 copy-start
  6.5 0.0 copy-start.1
  6.5 0.8 stack.16
  7.4 0.7 stack.17
  8.1 0.9 convolution_bitcast_fusion.4
  9.0 0.9 convolution_bitcast_fusion.3
  9.9 0.9 convolution_bitcast_fusion.2
  10.9 0.7 broadcast_in_dim.10
  11.5 13.7 %all-to-all-start = ((f32[32,3,2,128]{3,2,1,0:T(2,128)}), f32[32,3,2,128]{3,2,1,0:T(2,128)S(1)}, u32[]{:S(2)}, u32[]{:S(2)}) async-start(f32[32,3,2,128]{3,2,1,0:T(2,128)} %broadcast_in_dim.10), calls=%async_computation | async-start | bytes 196608 | tf_op jit(solution)/shard_map/all_to_all | solution.py:18
  26.9 1.0 fusion.45
  27.9 2.1 fusion
  30.0 0.7 convert_element_type.83
  30.7 3.7 %all-to-all-done = f32[32,3,2,128]{3,2,1,0:T(2,128)S(1)} async-done(((f32[32,3,2,128]{3,2,1,0:T(2,128)}), f32[32,3,2,128]{3,2,1,0:T(2,128)S(1)}, u32[]{:S(2)}, u32[]{:S(2)}) %all-to-all-start) | async-done | bytes 98336 | tf_op jit(solution)/shard_map/all_to_all | solution.py:18
  34.4 0.1 reduce_sum.36
  34.4 0.6 stack.23
  35.1 9.2 %all-to-all-start.1 = ((f32[16,3,2,128]{3,2,1,0:T(2,128)}), f32[16,3,2,128]{3,2,1,0:T(2,128)S(1)}, u32[]{:S(2)}, u32[]{:S(2)}) async-start(f32[16,3,2,128]{3,2,1,0:T(2,128)} %stack.23), calls=%async_computation.1 | async-start | bytes 98304 | tf_op jit(solution)/shard_map/all_to_all | solution.py:156
  44.3 0.0 all-reduce.6.cloned.1.call-start
  44.3 7.4 %all-to-all-done.1 = f32[16,3,2,128]{3,2,1,0:T(2,128)S(1)} async-done(((f32[16,3,2,128]{3,2,1,0:T(2,128)}), f32[16,3,2,128]{3,2,1,0:T(2,128)S(1)}, u32[]{:S(2)}, u32[]{:S(2)}) %all-to-all-start.1) | async-done | bytes 49184 | tf_op jit(solution)/shard_map/all_to_all | solution.py:156
  51.8 1.5 convolution_convert_fusion
  53.3 0.3 convolution_bitcast_fusion.1
  53.6 0.3 convolution_bitcast_fusion
  54.0 0.7 pad_maximum_fusion
  54.6 0.0 all-reduce.6.cloned.1.call-update
  54.7 0.0 reduce-scatter.2.cloned.1.call-start
  54.7 0.0 copy-done.1
  54.7 0.0 copy-done.8
  54.7 2.9 fusion.18
  57.6 0.0 copy-start.4
  57.6 0.1 fusion.53
  57.7 0.6 fusion.82
  58.3 0.0 copy-start.5
  58.3 0.0 copy-start.6
  58.3 0.0 copy-start.7
  58.3 0.3 fusion.40
  58.6 0.3 fusion.42
  58.9 9.7 %all-gather.4 = f32[4,129,128]{2,1,0:T(8,128)S(1)} all-gather(f32[1,129,128]{2,1,0:T(8,128)S(1)} %maximum_bitcast_fusion.4), channel_id=2, replica_groups=mesh['sp_0'=8,'sp_1'=4,'tp'=16] {'sp_1'}, dimensions={0}, use_global_device_ids=true | all-gather | bytes 330240 | tf_op jit(solution)/shard_map/all_gather | solution.py:49
  68.6 0.6 fusion.227
  72.4 10.4 %all-gather.6 = f32[4,129,128]{2,1,0:T(8,128)S(1)} all-gather(f32[1,129,128]{2,1,0:T(8,128)S(1)} %maximum_bitcast_fusion.6), channel_id=4, replica_groups=mesh['sp_0'=8,'sp_1'=4,'tp'=16] {'sp_1'}, dimensions={0}, use_global_device_ids=true | all-gather | bytes 330240 | tf_op jit(solution)/shard_map/all_gather | solution.py:49
  82.8 0.6 fusion.226
  87.7 2.0 fusion.233
  89.7 19.8 %all-gather.7 = f32[8,129,128]{2,1,0:T(8,128)S(1)} all-gather(f32[1,129,128]{2,1,0:T(8,128)S(1)} %maximum_bitcast_fusion.7), channel_id=5, replica_groups=mesh['sp_0'=8,'sp_1'=4,'tp'=16] {'sp_0'}, dimensions={0}, use_global_device_ids=true | all-gather | bytes 594432 | tf_op jit(solution)/shard_map/all_gather | solution.py:49
  109.5 0.7 fusion.224
  110.2 1.9 fusion.234
  112.1 19.8 %all-gather.5 = f32[8,129,128]{2,1,0:T(8,128)S(1)} all-gather(f32[1,129,128]{2,1,0:T(8,128)S(1)} %maximum_bitcast_fusion.5), channel_id=3, replica_groups=mesh['sp_0'=8,'sp_1'=4,'tp'=16] {'sp_0'}, dimensions={0}, use_global_device_ids=true | all-gather | bytes 594432 | tf_op jit(solution)/shard_map/all_gather | solution.py:49
  131.9 0.7 fusion.225
  133.8 0.0 copy-done.2
  133.8 0.0 copy-done.3
  133.8 1.5 convolution_multiply_fusion
  135.4 0.0 copy-done.4
  135.4 0.0 copy-done.5
  135.4 0.0 copy-done.6
  135.4 0.0 copy-done.7
  135.4 0.7 fusion.62
  136.1 59.5 %all-reduce.6.cloned.1.call-done = f32[32768]{0:T(1024)} async-done(((f32[32768]{0:T(1024)}), f32[32768]{0:T(1024)}) %all-reduce.6.cloned.1.call-update) | async-done | bytes 131088 | tf_op jit(solution)/shard_map/psum | solution.py:28
  195.7 7.9 %fusion.24 = f32[512,128]{0,1:T(8,128)S(1)} fusion(f32[512,128]{0,1:T(8,128)S(1)} %fusion.62, f32[512]{0:T(512)S(1)} %multiply_exponential_fusion.1, f32[32768]{0:T(1024)} %all-reduce.6.cloned.1.call-done, f32[8,129,128]{2,1,0:T(8,128)} %copy-done.3, f32[4,129,128]{2,1,0:T(8,128)S(1)} %all-gather.4, f32[512,1,32]{0,2,1:T(8,128)} %copy-done.5, ...), kind=kOutput, calls=%fused_computation.26 | convolution fusion | flops 101695488 | bytes 1847816 | tf_op jit(solution)/shard_map/htd,hde->hte/dot_general | solution.py:247
  203.6 7.9 %multiply_reduce_fusion = (f32[512]{0:T(512)S(1)}, f32[512,128]{0,1:T(8,128)S(1)}) fusion(f32[512,128]{0,1:T(8,128)S(1)} %fusion.24, f32[32768]{0:T(1024)} %all-reduce.6.cloned.1.call-done, f32[8,129,128]{2,1,0:T(8,128)} %copy-done.2, f32[4,129,128]{2,1,0:T(8,128)S(1)} %all-gather.6, f32[]{:T(128)} %bitcast.76, f32[]{:T(128)} %bitcast.77, f32[]{:T(128)} %bitcast.78, ...), kind=kOutput, calls=%fused_computation.53 | convolution fusion | flops 101826048 | bytes 1849864 | tf_op jit(solution)/shard_map/htd,hde->hte/dot_general | solution.py:250
  211.5 0.0 copy-done
  211.6 3.6 %fusion.50 = f32[512,2048]{1,0:T(8,128)} fusion(bf16[128,2048]{1,0:T(8,128)(2,1)S(1)} %copy-done, f32[512,128]{0,1:T(8,128)S(1)} %get-tuple-element.53, bf16[512,512]{0,1:T(8,128)(2,1)} %copy-done.4, f32[512]{0:T(512)S(1)} %add_rsqrt_fusion), kind=kOutput, calls=%fused_computation.66 | convolution fusion | flops 268959744 | bytes 5113856 | tf_op jit(solution)/shard_map/dot_general | solution.py:256
  215.2 0.0 reduce-scatter.2.cloned.1.call-update
  215.2 66.1 %reduce-scatter.2.cloned.1.call-done = f32[32,2048]{1,0:T(8,128)} async-done(((f32[512,2048]{1,0:T(8,128)}), f32[32,2048]{1,0:T(8,128)}) %reduce-scatter.2.cloned.1.call-update) | async-done | bytes 262160 | tf_op jit(solution)/shard_map/reduce_scatter | solution.py:255
  281.4 1.0 add_convert_fusion
  282.3 0.2 broadcast_in_dim.12
  282.6 57.6 %all_to_all.15 = bf16[16,32,2048]{2,1,0:T(8,128)(2,1)S(1)} all-to-all(bf16[16,32,2048]{2,1,0:T(8,128)(2,1)S(1)} %broadcast_in_dim.12), channel_id=1, replica_groups=mesh['sp_0'=8,'sp_1'=4,'tp'=16] {'tp'}, dimensions={0} | all-to-all | bytes 4194304 | tf_op jit(solution)/shard_map/all_to_all | solution.py:18
  340.2 1.3 copy.47
  (29 shorter events, 0.2 us)
Async XLA Ops:
  6.5 205.0 %copy-start = (bf16[128,2048]{1,0:T(8,128)(2,1)S(1)}, bf16[128,2048]{1,0:T(8,128)(2,1)}, u32[]{:S(2)}) copy-start(bf16[128,2048]{1,0:T(8,128)(2,1)} %param.29) | copy-start | bytes 1572868
  6.5 48.2 %copy-start.1 = (bf16[512,2048]{1,0:T(8,128)(2,1)S(1)}, bf16[512,2048]{1,0:T(8,128)(2,1)}, u32[]{:S(2)}) copy-start(bf16[512,2048]{1,0:T(8,128)(2,1)} %param.15) | copy-start | bytes 6291460
  6.5 48.2 %copy-start.8 = (bf16[2048,128]{1,0:T(8,128)(2,1)S(1)}, bf16[2048,128]{1,0:T(8,128)(2,1)}, u32[]{:S(2)}) copy-start(bf16[2048,128]{1,0:T(8,128)(2,1)} %param.25) | copy-start | bytes 1572868
  11.5 22.8 %all-to-all-start = ((f32[32,3,2,128]{3,2,1,0:T(2,128)}), f32[32,3,2,128]{3,2,1,0:T(2,128)S(1)}, u32[]{:S(2)}, u32[]{:S(2)}) async-start(f32[32,3,2,128]{3,2,1,0:T(2,128)} %broadcast_in_dim.10), calls=%async_computation | async-start | bytes 196608 | tf_op jit(solution)/shard_map/all_to_all | solution.py:18
  35.1 16.7 %all-to-all-start.1 = ((f32[16,3,2,128]{3,2,1,0:T(2,128)}), f32[16,3,2,128]{3,2,1,0:T(2,128)S(1)}, u32[]{:S(2)}, u32[]{:S(2)}) async-start(f32[16,3,2,128]{3,2,1,0:T(2,128)} %stack.23), calls=%async_computation.1 | async-start | bytes 98304 | tf_op jit(solution)/shard_map/all_to_all | solution.py:156
  44.3 151.4 %all-reduce.6.cloned.1.call-start = ((), (), s32[]{:S(2)}) async-start(), calls=%async_computation.4 | async-start | bytes 262144 | tf_op jit(solution)/shard_map/psum | solution.py:28
  54.7 226.7 %reduce-scatter.2.cloned.1.call-start = ((), (), s32[]{:S(2)}) async-start(), calls=%async_computation.5 | async-start | bytes 4456448 | tf_op jit(solution)/shard_map/reduce_scatter | solution.py:255
  57.6 77.8 %copy-start.4 = (bf16[512,512]{0,1:T(8,128)(2,1)}, bf16[512,512]{0,1:T(8,128)(2,1)S(1)}, u32[]{:S(2)}) copy-start(bf16[512,512]{0,1:T(8,128)(2,1)S(1)} %fusion.18) | copy-start | bytes 1572868
  58.3 77.1 %copy-start.5 = (f32[512,1,32]{0,2,1:T(8,128)}, f32[512,1,32]{0,2,1:T(8,128)S(1)}, u32[]{:S(2)}) copy-start(f32[512,1,32]{0,2,1:T(8,128)S(1)} %get-tuple-element.25) | copy-start | bytes 196612
  58.3 77.1 %copy-start.6 = (f32[512,1,32]{0,2,1:T(8,128)}, f32[512,1,32]{0,2,1:T(8,128)S(1)}, u32[]{:S(2)}) copy-start(f32[512,1,32]{0,2,1:T(8,128)S(1)} %get-tuple-element.26) | copy-start | bytes 196612
  58.3 77.1 %copy-start.7 = (f32[512,1,32]{0,2,1:T(8,128)}, f32[512,1,32]{0,2,1:T(8,128)S(1)}, u32[]{:S(2)}) copy-start(f32[512,1,32]{0,2,1:T(8,128)S(1)} %get-tuple-element.27) | copy-start | bytes 196612
  109.5 24.3 %copy-start.2 = (f32[8,129,128]{2,1,0:T(8,128)}, f32[8,129,128]{2,1,0:T(8,128)S(1)}, u32[]{:S(2)}) copy-start(f32[8,129,128]{2,1,0:T(8,128)S(1)} %all-gather.7) | copy-start | bytes 1585156
  131.9 2.0 copy-start.3
Sparse Core Ops, SparseCore 0:
  54.8 140.8 all-reduce.5
  215.3 65.9 reduce-scatter.1
